TPU v7x, 32 devices: a whole 2x2x4 slice. The times are simulated.
32 devices in a mesh: sp: 8 (over z, y), tp: 4 (over x, core).
Axes of the slice: x: 2, y: 2, z: 4, core: 2. Of those that a mesh axis runs over, the one named last changes fastest.
Arguments:
- tokens: bfloat16 [1024, 2048], P(('sp', 'tp')), may hold values from -64 to 64, as said below
- query_one: bfloat16 [2048, 256], P(None, 'tp'), may hold values from -0.125 to 0.125
- query_two: bfloat16 [2048, 256], P(None, 'tp'), may hold values from -0.125 to 0.125
- key_one: bfloat16 [2048, 256], P(None, 'tp'), may hold values from -0.125 to 0.125
- key_two: bfloat16 [2048, 256], P(None, 'tp'), may hold values from -0.125 to 0.125
- value_weight: bfloat16 [2048, 512], P(None, 'tp'), may hold values from -0.125 to 0.125
- mixing: float32 [4], P('tp'), may hold values from 0.3 to 0.8
- out_weight: bfloat16 [512, 2048], replicated, may hold values from -0.25 to 0.25
- head_gain: float32 [128], replicated, may hold values from 0.1 to 1.9
Outputs:
- attended: bfloat16 [1024, 2048], P(('sp', 'tp'))
Inputs may be any that keep to these rules, and one draw needn't show every extreme that they name: `tokens`: Real-valued activations.
All inputs are finite; a program needn't handle non-finite values.
Results may differ from a plain program's by a relative error of at most 0.012.
The roundings to bfloat16 on the way count: a program that leaves them out, or rounds other values in their place, can miss the bound.
Values may be sent and summed in bfloat16 or wider, within the bound.
A program may use at most 64 MiB of HBM per device.

v0:
```python
import math

import jax
import jax.numpy as jnp
from jax import lax
from jax.sharding import PartitionSpec as P

HEAD = 64
GRID_W = 64


epsilon = 1e-06
theta_base = 10000.0
floor_value = -1e30


def grid_turn(field, positions):
    quarter = field.shape[-1] // 4
    half = 2 * quarter
    freqs = theta_base ** (-jnp.arange(quarter, dtype=jnp.float32) / quarter)
    row_angle = (positions // GRID_W).astype(jnp.float32)[:, None] * freqs
    col_angle = (positions % GRID_W).astype(jnp.float32)[:, None] * freqs

    def turn(segment, angle):
        cosine = jnp.cos(angle)[:, None, :]
        sine = jnp.sin(angle)[:, None, :]
        first = segment[..., :quarter]
        second = segment[..., quarter:]
        return jnp.concatenate(
            [first * cosine - second * sine, first * sine + second * cosine], axis=-1
        )

    return jnp.concatenate(
        [turn(field[..., :half], row_angle), turn(field[..., half:], col_angle)], axis=-1
    )


def one_map(state, queries, keys, values):
    peak, total, summed = state
    scores = jnp.einsum(
        "qhd,khd->qhk", queries, keys, preferred_element_type=jnp.float32
    ) * HEAD ** (-0.5)
    new_peak = jnp.maximum(peak, jnp.max(scores, axis=-1))
    factor = jnp.exp(peak - new_peak)
    weights = jnp.exp(scores - new_peak[..., None])
    total = total * factor + jnp.sum(weights, axis=-1)
    summed = summed * factor[..., None] + jnp.einsum(
        "qhk,khe->qhe", weights.astype(jnp.bfloat16), values, preferred_element_type=jnp.float32
    )
    return (new_peak, total, summed)


def make_absorb(q_first, q_second, head_local):
    cols = head_local * HEAD

    def absorb(carry, piece, start):
        count = piece.shape[0]
        width = math.gcd(count, 2048)

        def step(index, state):
            block = lax.dynamic_slice_in_dim(piece, index * width, width, 0)
            keys_first = block[:, :cols].reshape(width, head_local, HEAD)
            keys_second = block[:, cols : 2 * cols].reshape(width, head_local, HEAD)
            values = block[:, 2 * cols :].reshape(width, head_local, 2 * HEAD)
            return (
                one_map(state[0], q_first, keys_first, values),
                one_map(state[1], q_second, keys_second, values),
            )

        return lax.fori_loop(0, count // width, step, carry)

    return absorb


def per_device(
    tokens, query_one, query_two, key_one, key_two, value_weight, mixing, out_weight, head_gain
):
    groups = lax.axis_size("tp")
    own_rows = tokens.shape[0]
    row_count = own_rows * groups
    head_cols = query_one.shape[1]
    head_local = head_cols // HEAD
    joined = jnp.concatenate([query_one, query_two, key_one, key_two, value_weight], axis=1)
    projected = jnp.dot(
        lax.all_gather(tokens, "tp", axis=0, tiled=True), joined, preferred_element_type=jnp.float32
    )
    positions = lax.axis_index("sp") * row_count + jnp.arange(row_count, dtype=jnp.int32)

    def heads_of(lower, upper):
        return projected[:, lower:upper].reshape(row_count, head_local, HEAD)

    q_first = grid_turn(heads_of(0, head_cols), positions).astype(jnp.bfloat16)
    q_second = grid_turn(heads_of(head_cols, 2 * head_cols), positions).astype(jnp.bfloat16)
    k_first = grid_turn(heads_of(2 * head_cols, 3 * head_cols), positions).astype(jnp.bfloat16)
    k_second = grid_turn(heads_of(3 * head_cols, 4 * head_cols), positions).astype(jnp.bfloat16)
    values = projected[:, 4 * head_cols :].astype(jnp.bfloat16)
    packed = jnp.concatenate(
        [k_first.reshape(row_count, head_cols), k_second.reshape(row_count, head_cols), values],
        axis=1,
    )
    absorb = make_absorb(q_first, q_second, head_local)
    empty = (
        jnp.full((row_count, head_local), floor_value, jnp.float32),
        jnp.zeros((row_count, head_local), jnp.float32),
        jnp.zeros((row_count, head_local, 2 * HEAD), jnp.float32),
    )
    gathered = lax.all_gather(packed, "sp", axis=0, tiled=True)
    first_map, second_map = absorb((empty, empty), gathered, 0)
    mixed = first_map[2] / first_map[1][..., None] - mixing[None, :, None] * (
        second_map[2] / second_map[1][..., None]
    )
    normed = (
        mixed * lax.rsqrt(jnp.mean(mixed * mixed, axis=-1, keepdims=True) + epsilon) * head_gain
    )
    heads = normed.astype(jnp.bfloat16).reshape(row_count, head_local * 2 * HEAD)
    regrouped = lax.all_to_all(heads, "tp", split_axis=0, concat_axis=1, tiled=True)
    summed = jnp.dot(regrouped, out_weight, preferred_element_type=jnp.float32)
    return summed.astype(jnp.bfloat16)


def solution(mesh):
    in_specs = (
        P(("sp", "tp"), None),
        P(None, "tp"),
        P(None, "tp"),
        P(None, "tp"),
        P(None, "tp"),
        P(None, "tp"),
        P("tp"),
        P(),
        P(),
    )
    out_specs = P(("sp", "tp"), None)
    return jax.shard_map(
        per_device, mesh=mesh, in_specs=in_specs, out_specs=out_specs, check_vma=False
    )
```

profile of v0, /device:TPU:0, one launch (start us, length us, event | category | flops | bytes accessed | tf_op | source)
XLA Modules:
  0.0 59.8 jit_solution(14919113349166023938)
XLA Ops:
  0.0 0.0 copy-start
  0.0 0.0 copy-start.1
  0.0 0.0 copy-start.2
  0.0 1.4 %copy.19 = bf16[2048,64]{1,0:T(8,128)(2,1)S(1)} copy(bf16[2048,64]{0,1:T(8,128)(2,1)} %param.10) | data formatting | bytes 524288 | tf_op args[1]
  1.4 2.0 %copy.20 = bf16[2048,64]{1,0:T(8,128)(2,1)} copy(bf16[2048,64]{0,1:T(8,128)(2,1)} %param.11) | data formatting | bytes 524288 | tf_op args[2]
  3.4 2.0 %copy.21 = bf16[2048,64]{1,0:T(8,128)(2,1)} copy(bf16[2048,64]{0,1:T(8,128)(2,1)} %param.12) | data formatting | bytes 524288 | tf_op args[3]
  5.3 0.0 copy-done.1
  5.3 1.0 %copy.22 = bf16[2048,64]{1,0:T(8,128)(2,1)} copy(bf16[2048,64]{0,1:T(8,128)(2,1)S(1)} %copy-done.1) | data formatting | bytes 524288 | tf_op args[4]
  6.4 0.0 copy-done.2
  6.4 8.6 %all_gather.6 = bf16[128,2048]{1,0:T(8,128)(2,1)S(1)} all-gather(bf16[32,2048]{1,0:T(8,128)(2,1)S(1)} %copy-done.2), channel_id=1, replica_groups=mesh['sp'=8,'tp'=4] {'tp'}, dimensions={0}, use_global_device_ids=true | all-gather | bytes 655360 | tf_op jit(solution)/shard_map/all_gather | solution.py:85
  15.0 4.1 %concatenate.63 = bf16[2048,384]{1,0:T(8,128)(2,1)} concatenate(bf16[2048,64]{1,0:T(8,128)(2,1)S(1)} %copy.19, bf16[2048,64]{1,0:T(8,128)(2,1)} %copy.20, bf16[2048,64]{1,0:T(8,128)(2,1)} %copy.21, bf16[2048,64]{1,0:T(8,128)(2,1)} %copy.22, bf16[2048,128]{1,0:T(8,128)(2,1)} %param.14), dimensions={1} | concatenate | bytes 3145728 | tf_op jit(solution)/shard_map/concatenate | solution.py:83
  19.1 2.0 %convolution_bitcast_fusion = f32[128,384]{0,1:T(8,128)S(1)} fusion(bf16[2048,384]{1,0:T(8,128)(2,1)} %concatenate.63, bf16[128,2048]{1,0:T(8,128)(2,1)S(1)} %all_gather.6), kind=kOutput, calls=%fused_computation.3 | convolution fusion | flops 201326592 | bytes 2293760 | tf_op jit(solution)/shard_map/dot_general | solution.py:84
  21.2 0.1 constant_dynamic-update-slice_fusion.7
  21.3 0.1 constant_dynamic-update-slice_fusion.6
  21.4 0.1 constant_dynamic-update-slice_fusion.5
  21.5 0.1 constant_dynamic-update-slice_fusion.4
  21.7 0.1 constant_dynamic-update-slice_fusion.3
  21.8 0.1 constant_dynamic-update-slice_fusion.2
  21.9 0.1 constant_dynamic-update-slice_fusion.1
  22.1 0.1 constant_dynamic-update-slice_fusion
  22.2 27.5 %all_gather.7 = bf16[1024,256]{0,1:T(8,128)(2,1)S(1)} all-gather(bf16[128,256]{0,1:T(8,128)(2,1)S(1)} %fusion.22), channel_id=1, replica_groups=mesh['sp'=8,'tp'=4] {'sp'}, dimensions={0}, use_global_device_ids=true | all-gather | bytes 589824 | tf_op jit(solution)/shard_map/all_gather | solution.py:107
  49.7 0.2 fusion.108
  49.8 0.0 copy-start.3
  49.8 0.3 fusion.117
  50.2 0.2 fusion.10
  51.0 0.3 fusion.118
  51.4 0.2 fusion.8
  51.5 0.3 fusion.5
  51.8 0.4 multiply_reduce_fusion
  52.2 0.0 copy-done.3
  52.2 0.1 multiply_convert_fusion
  52.3 6.3 %all_to_all.19 = bf16[4,32,128]{2,1,0:T(8,128)(2,1)S(1)} all-to-all(bf16[4,32,128]{2,1,0:T(8,128)(2,1)S(1)} %bitcast.110), channel_id=1, replica_groups=mesh['sp'=8,'tp'=4] {'tp'}, dimensions={0} | all-to-all | bytes 65536 | tf_op jit(solution)/shard_map/all_to_all | solution.py:116
  58.6 0.0 copy-done
  58.6 1.1 %convolution_convert_fusion = bf16[32,2048]{1,0:T(8,128)(2,1)} fusion(bf16[512,2048]{1,0:T(8,128)(2,1)S(1)} %copy-done, bf16[4,32,128]{2,1,0:T(8,128)(2,1)S(1)} %all_to_all.19), kind=kOutput, calls=%fused_computation | convolution fusion | flops 67174400 | bytes 2260992 | tf_op jit(solution)/shard_map/dot_general | solution.py:117
  (9 shorter events, 0.1 us)
Async XLA Ops:
  0.0 58.6 %copy-start = (bf16[512,2048]{1,0:T(8,128)(2,1)S(1)}, bf16[512,2048]{1,0:T(8,128)(2,1)}, u32[]{:S(2)}) copy-start(bf16[512,2048]{1,0:T(8,128)(2,1)} %param.16) | copy-start | bytes 6291460
  0.0 5.3 %copy-start.1 = (bf16[2048,64]{0,1:T(8,128)(2,1)S(1)}, bf16[2048,64]{0,1:T(8,128)(2,1)}, u32[]{:S(2)}) copy-start(bf16[2048,64]{0,1:T(8,128)(2,1)} %param.13) | copy-start | bytes 786436
  0.0 6.4 %copy-start.2 = (bf16[32,2048]{1,0:T(8,128)(2,1)S(1)}, bf16[32,2048]{1,0:T(8,128)(2,1)}, u32[]{:S(2)}) copy-start(bf16[32,2048]{1,0:T(8,128)(2,1)} %param.9) | copy-start | bytes 393220
  49.8 2.4 %copy-start.3 = (f32[128]{0:T(128)S(1)}, f32[128]{0:T(128)}, u32[]{:S(2)}) copy-start(f32[128]{0:T(128)} %param.17) | copy-start | bytes 1540
where the time goes:
time: 60.1 us; the launch traced here: 59.8 us
  blocking collectives  42.4 us (71%)
  local copies, waits for them, and re-layouts  10.5 us (17%)
  matrix products  4.48 us (7%)
  other arithmetic  1.64 us (3%)
  between operations  0.75 us (1%)
    all_gather x1, blocking collectives, per_device(): gathered = lax.all_gather(packed, 'sp', axis=0, tiled=True)  27.5 us
    all_gather x1, blocking collectives, per_device(): lax.all_gather(tokens, 'tp', axis=0, tiled=True)  8.64 us
    unnamed x12, local copies, waits for them, and re-layouts  6.35 us
    all_to_all x1, blocking collectives, per_device(): lax.all_to_all(heads, 'tp', split_axis=0, concat_axis=1, tiled=True)  6.3 us
    concatenate x1, local copies, waits for them, and re-layouts, per_device(): jnp.concatenate([query_one, query_two, key_one, key_two, value_weight], a...  4.1 us
    dot_general x1, matrix products, per_device(): jnp.dot(lax.all_gather(tokens, 'tp', axis=0, tiled=True), joined, preferr...  2.01 us

commit v1 on v0

v1 whole, which is shorter than its diff:
```python
import functools
import math

import jax
import jax.numpy as jnp
from jax import lax
from jax.experimental import pallas as pl
from jax.experimental.pallas import tpu as pltpu
from jax.sharding import PartitionSpec as P

HEAD = 64
GRID_W = 64
QUARTER = HEAD // 4

epsilon = 1e-06
theta_base = 10000.0
floor_value = -1e30
MESH = pl.DeviceIdType.MESH
NT = (((1,), (1,)), ((), ()))
CHUNKS = 4


def rotary_tables(start, rows):
    shape = (rows, 2 * HEAD)
    lane = lax.broadcasted_iota(jnp.int32, shape, 1)
    token = lax.broadcasted_iota(jnp.int32, shape, 0) + start
    entry = lane % QUARTER
    freqs = jnp.zeros(shape, jnp.float32)
    for j in range(QUARTER):
        freqs = jnp.where(entry == j, jnp.float32(theta_base ** (-j / QUARTER)), freqs)
    by_row = (lane % HEAD) < 2 * QUARTER
    position = jnp.where(by_row, token // GRID_W, token % GRID_W).astype(jnp.float32)
    angle = position * freqs
    first = (lane % (2 * QUARTER)) < QUARTER
    sine = jnp.sin(angle)
    return jnp.cos(angle), jnp.where(first, -sine, sine)


def turn(field, cosine, sine):
    lane = lax.broadcasted_iota(jnp.int32, field.shape, 1)
    first = (lane % (2 * QUARTER)) < QUARTER
    width = field.shape[1]
    other = jnp.where(
        first, pltpu.roll(field, width - QUARTER, 1), pltpu.roll(field, QUARTER, 1)
    )
    return field * cosine + other * sine


def kernel(
    sp, tp,
    tokens, wq1, wq2, wk1, wk2, wv, mixing, wo, gain, out,
    tok, wqk, wvv, wov, tables, kv, hsend, hrecv,
    load_sems, tsend, trecv, fsend, frecv, ksend, krecv, hs_sems, hr_sems,
):
    own_rows, depth = tokens.shape
    rows = own_rows * tp
    groups = tp // 2
    me_tp = lax.axis_index("tp")
    me_sp = lax.axis_index("sp")
    partner = me_tp + 1 - 2 * (me_tp % 2)
    span = depth // CHUNKS

    tok_load = pltpu.make_async_copy(tokens, tok.at[me_tp], load_sems.at[0])
    tok_load.start()
    loads = []
    for i, w in enumerate((wq1, wq2, wk1, wk2)):
        loads.append(pltpu.make_async_copy(w, wqk.at[pl.ds(i * HEAD, HEAD)], load_sems.at[1 + i]))
    loads.append(pltpu.make_async_copy(wv, wvv, load_sems.at[5]))
    for c in loads:
        c.start()
    wo_load = pltpu.make_async_copy(wo, wov, load_sems.at[6])
    wo_load.start()

    barrier = pltpu.get_barrier_semaphore()
    for d in range(1, tp):
        pl.semaphore_signal(barrier, inc=1, device_id={"tp": lax.rem(me_tp + d, tp)}, device_id_type=MESH)

    def greet(d, _):
        pl.semaphore_signal(barrier, inc=1, device_id={"sp": lax.rem(me_sp + d, sp)}, device_id_type=MESH)
        return _

    lax.fori_loop(1, sp, greet, 0)
    pl.semaphore_wait(barrier, tp - 1 + sp - 1)

    def part(slot, c):
        return tok.at[slot, :, pl.ds(c * span, span)]

    def send(slot, c, target, s_sem, r_sem):
        return pltpu.make_async_remote_copy(
            src_ref=part(slot, c), dst_ref=part(slot, c), send_sem=s_sem, recv_sem=r_sem,
            device_id={"tp": target}, device_id_type=MESH,
        )

    def peer(g):
        return lax.rem(me_tp + 2 * g, tp)

    tok_load.wait()
    first_sends, forwards = [], []
    for c in range(CHUNKS):
        for g in range(1, groups):
            cp = send(me_tp, c, peer(g), tsend.at[g, c], trecv.at[g, c])
            cp.start()
            first_sends.append(cp)
        cp = send(me_tp, c, partner, tsend.at[0, c], trecv.at[0, c])
        cp.start()
        first_sends.append(cp)

    cosine, sine = rotary_tables(me_sp * rows, rows)
    tables[0] = cosine
    tables[1] = sine
    for c in loads:
        c.wait()

    acc_qk = jnp.zeros((rows, 4 * HEAD), jnp.float32)
    acc_v = jnp.zeros((rows, 2 * HEAD), jnp.float32)
    for c in range(CHUNKS):
        for g in range(1, groups):
            slot = lax.rem(me_tp + tp - 2 * g, tp)
            send(slot, c, partner, tsend.at[g, c], trecv.at[g, c]).wait_recv()
            cp = send(slot, c, partner, fsend.at[g, c], frecv.at[g, c])
            cp.start()
            forwards.append(cp)
        send(partner, c, partner, tsend.at[0, c], trecv.at[0, c]).wait_recv()
        for g in range(1, groups):
            slot = lax.rem(partner + tp - 2 * g, tp)
            send(slot, c, partner, fsend.at[g, c], frecv.at[g, c]).wait_recv()
        x = tok[:, :, c * span:(c + 1) * span].reshape(rows, span)
        acc_qk += lax.dot_general(x, wqk[:, c * span:(c + 1) * span], NT, preferred_element_type=jnp.float32)
        acc_v += jnp.dot(x, wvv[c * span:(c + 1) * span, :], preferred_element_type=jnp.float32)

    cosine, sine = tables[0], tables[1]
    keys = turn(acc_qk[:, 2 * HEAD:], cosine, sine).astype(jnp.bfloat16)
    kv[me_sp, :, : 2 * HEAD] = keys
    kv[me_sp, :, 2 * HEAD :] = acc_v.astype(jnp.bfloat16)

    def kv_copy(slot, d, target):
        return pltpu.make_async_remote_copy(
            src_ref=kv.at[slot], dst_ref=kv.at[slot], send_sem=ksend.at[d], recv_sem=krecv.at[d],
            device_id={"sp": target}, device_id_type=MESH,
        )

    def start_kv(d, _):
        kv_copy(me_sp, d, lax.rem(me_sp + d, sp)).start()
        return _

    lax.fori_loop(1, sp, start_kv, 0)

    queries = turn(acc_qk[:, : 2 * HEAD], cosine, sine)
    lane = lax.broadcasted_iota(jnp.int32, queries.shape, 1)
    both = jnp.concatenate(
        [jnp.where(lane < HEAD, queries, 0.0), jnp.where(lane < HEAD, 0.0, queries)], axis=0
    ).astype(jnp.bfloat16)

    def absorb(slot, state):
        peak, total, summed = state
        k = kv[slot, :, : 2 * HEAD]
        v = kv[slot, :, 2 * HEAD :]
        scores = lax.dot_general(both, k, NT, preferred_element_type=jnp.float32) * HEAD ** (-0.5)
        new_peak = jnp.maximum(peak, jnp.max(scores, axis=1, keepdims=True))
        factor = jnp.exp(peak - new_peak)
        weights = jnp.exp(scores - new_peak)
        total = total * factor + jnp.sum(weights, axis=1, keepdims=True)
        summed = summed * factor + jnp.dot(
            weights.astype(jnp.bfloat16), v, preferred_element_type=jnp.float32
        )
        return new_peak, total, summed

    state = (
        jnp.full((2 * rows, 1), floor_value, jnp.float32),
        jnp.zeros((2 * rows, 1), jnp.float32),
        jnp.zeros((2 * rows, 2 * HEAD), jnp.float32),
    )
    state = absorb(me_sp, state)

    def step(d, state):
        slot = lax.rem(me_sp + sp - d, sp)
        kv_copy(slot, d, slot).wait_recv()
        return absorb(slot, state)

    if sp <= 16:
        for d in range(1, sp):
            state = step(d, state)
    else:
        state = lax.fori_loop(1, sp, step, state)

    _, total, summed = state
    ratio = summed / total
    mixed = ratio[:rows] - mixing[0] * ratio[rows:]
    normed = (
        mixed * lax.rsqrt(jnp.mean(mixed * mixed, axis=-1, keepdims=True) + epsilon) * gain[...]
    )
    hsend[...] = normed.astype(jnp.bfloat16).reshape(tp, own_rows, 2 * HEAD)
    head_sends = []
    for d in range(1, tp):
        target = lax.rem(me_tp + d, tp)
        cp = pltpu.make_async_remote_copy(
            src_ref=hsend.at[target], dst_ref=hrecv.at[me_tp],
            send_sem=hs_sems.at[d], recv_sem=hr_sems.at[d],
            device_id={"tp": target}, device_id_type=MESH,
        )
        cp.start()
        head_sends.append(cp)
    hrecv[me_tp] = hsend[me_tp]
    wo_load.wait()
    for cp in head_sends:
        cp.wait_recv()
    joined = jnp.concatenate([hrecv[h] for h in range(tp)], axis=1)
    out[...] = jnp.dot(joined, wov[...], preferred_element_type=jnp.float32).astype(out.dtype)

    for cp in first_sends + forwards + head_sends:
        cp.wait_send()

    def drain(d, _):
        kv_copy(me_sp, d, lax.rem(me_sp + d, sp)).wait_send()
        return _

    lax.fori_loop(1, sp, drain, 0)


def per_device(
    sp, tp,
    tokens, query_one, query_two, key_one, key_two, value_weight, mixing, out_weight, head_gain
):
    own_rows, depth = tokens.shape
    rows = own_rows * tp
    assert query_one.shape[1] == HEAD
    any_spec = pl.BlockSpec(memory_space=pl.ANY)
    vmem = pl.BlockSpec(memory_space=pltpu.VMEM)
    dma = pltpu.SemaphoreType.DMA
    bf16 = jnp.bfloat16
    return pl.pallas_call(
        functools.partial(kernel, sp, tp),
        out_shape=jax.ShapeDtypeStruct((own_rows, out_weight.shape[1]), bf16),
        in_specs=[any_spec] * 6 + [pl.BlockSpec(memory_space=pltpu.SMEM), any_spec, vmem],
        out_specs=vmem,
        scratch_shapes=[
            pltpu.VMEM((tp, own_rows, depth), bf16),
            pltpu.VMEM((4 * HEAD, depth), bf16),
            pltpu.VMEM((depth, 2 * HEAD), bf16),
            pltpu.VMEM(out_weight.shape, bf16),
            pltpu.VMEM((2, rows, 2 * HEAD), jnp.float32),
            pltpu.VMEM((sp, rows, 4 * HEAD), bf16),
            pltpu.VMEM((tp, own_rows, 2 * HEAD), bf16),
            pltpu.VMEM((tp, own_rows, 2 * HEAD), bf16),
            dma((7,)),
            dma((tp // 2, CHUNKS)),
            dma((tp // 2, CHUNKS)),
            dma((tp // 2, CHUNKS)),
            dma((tp // 2, CHUNKS)),
            dma((sp,)),
            dma((sp,)),
            dma((tp,)),
            dma((tp,)),
        ],
        compiler_params=pltpu.CompilerParams(
            collective_id=0, has_side_effects=True, vmem_limit_bytes=56 * 1024 * 1024
        ),
    )(
        tokens, query_one.T, query_two.T, key_one.T, key_two.T, value_weight,
        mixing, out_weight, head_gain.reshape(1, -1),
    )


def solution(mesh):
    in_specs = (
        P(("sp", "tp"), None),
        P(None, "tp"),
        P(None, "tp"),
        P(None, "tp"),
        P(None, "tp"),
        P(None, "tp"),
        P("tp"),
        P(),
        P(),
    )
    out_specs = P(("sp", "tp"), None)
    return jax.shard_map(
        functools.partial(per_device, mesh.shape["sp"], mesh.shape["tp"]),
        mesh=mesh, in_specs=in_specs, out_specs=out_specs, check_vma=False,
    )
```

time: 60.1 us -> 32.7 us (0.54)
  blocking collectives: 42.4 us -> 0 us
  Pallas kernels: 0 us -> 30.3 us
  local copies, waits for them, and re-layouts: 10.5 us -> 1.57 us
  matrix products: 4.48 us -> 0 us
  other arithmetic: 1.64 us -> 0 us
    all_gather x2 -> x0, blocking collectives: 36.1 us -> none  [the longest x1 27.5 us: per_device(): gathered = lax.all_gather(packed, 'sp', axis=0, tiled=True)]
    pallas_call x0 -> x1, Pallas kernels: none -> 30.3 us  [per_device(): pl.pallas_call(functools.partial(kernel, sp, tp), out_shape=jax.ShapeDtyp...]
    all_to_all x1 -> x0, blocking collectives: 6.3 us -> none  [per_device(): lax.all_to_all(heads, 'tp', split_axis=0, concat_axis=1, tiled=True)]
    unnamed x12 -> x1, local copies, waits for them, and re-layouts: 6.35 us -> 1.57 us
    dot_general x6 -> x0, matrix products: 4.48 us -> none  [the longest x1 2.01 us: per_device(): jnp.dot(lax.all_gather(tokens, 'tp', axis=0, tiled=True), joined, preferr...]
    concatenate x2 -> x0, local copies, waits for them, and re-layouts: 4.11 us -> none  [the longest x1 4.1 us: per_device(): jnp.concatenate([query_one, query_two, key_one, key_two, value_weight], a...]
    unnamed x8 -> x0, other arithmetic: 1.02 us -> none
where the time goes in v1:
time: 32.7 us; the launch traced here: 32.5 us
  Pallas kernels  30.3 us (93%)
  local copies, waits for them, and re-layouts  1.57 us (5%)
  between operations  0.66 us (2%)
    pallas_call x1, Pallas kernels, per_device(): pl.pallas_call(functools.partial(kernel, sp, tp), out_shape=jax.ShapeDtyp...  30.3 us
    unnamed x1, local copies, waits for them, and re-layouts  1.57 us

profile of v1, /device:TPU:0, one launch (start us, length us, event | category | flops | bytes accessed | tf_op | source)
XLA Modules:
  0.0 32.5 jit_solution(14721793490758169240)
XLA Ops:
  0.7 30.3 %shard_map.91 = bf16[32,2048]{1,0:T(8,128)(2,1)} custom-call(bf16[32,2048]{1,0:T(8,128)(2,1)} %tokens.1, bf16[64,2048]{1,0:T(8,128)(2,1)} %bitcast.5, bf16[64,2048]{1,0:T(8,128)(2,1)} %bitcast.6, bf16[64,2048]{1,0:T(8,128)(2,1)} %bitcast.7, bf16[64,2048]{1,0:T(8,128)(2,1)} %bitcast.8, bf16[2048,128]{1,0:T(8,128)(2,1)} %wv.1, f32[1]{0:T(128)S(6)} %copy.11.mixing, ...), custom_call_target="tpu_custom_call" | custom-call | tf_op jit(solution)/shard_map/pallas_call | solution.py:231
  30.9 1.6 %copy.12 = bf16[32,2048]{1,0:T(8,128)(2,1)} copy(bf16[32,2048]{1,0:T(8,128)(2,1)} %shard_map.91) | data formatting | bytes 262144

commit v2 on v1

--- a/solution.py
+++ b/solution.py
@@ -49,8 +49,8 @@
 def kernel(
     sp, tp,
     tokens, wq1, wq2, wk1, wk2, wv, mixing, wo, gain, out,
-    tok, wqk, wvv, wov, tables, kv, hsend, hrecv,
-    load_sems, tsend, trecv, fsend, frecv, ksend, krecv, hs_sems, hr_sems,
+    tok, wqk, wvv, wov, tables, kv, qbuf, hsend, hrecv,
+    load_sems, tsend, trecv, fsend, frecv, ksend, krecv, hs_sems, hr_sems, ready,
 ):
     own_rows, depth = tokens.shape
     rows = own_rows * tp
@@ -71,24 +71,39 @@
     wo_load = pltpu.make_async_copy(wo, wov, load_sems.at[6])
     wo_load.start()
 
+    depth_z = sp // 2
+    me_z = me_sp // 2
+    side = me_sp + 1 - 2 * (me_sp % 2)
     barrier = pltpu.get_barrier_semaphore()
+    has_left = jnp.minimum(me_z, 1)
+    has_right = jnp.minimum(depth_z - 1 - me_z, 1)
+
+    def signal_line(left_sem, right_sem):
+        @pl.when(me_z > 0)
+        def _():
+            pl.semaphore_signal(right_sem, inc=1, device_id={"sp": me_sp - 2}, device_id_type=MESH)
+
+        @pl.when(me_z < depth_z - 1)
+        def _():
+            pl.semaphore_signal(left_sem, inc=1, device_id={"sp": me_sp + 2}, device_id_type=MESH)
+
     for d in range(1, tp):
         pl.semaphore_signal(barrier, inc=1, device_id={"tp": lax.rem(me_tp + d, tp)}, device_id_type=MESH)
-
-    def greet(d, _):
-        pl.semaphore_signal(barrier, inc=1, device_id={"sp": lax.rem(me_sp + d, sp)}, device_id_type=MESH)
-        return _
-
-    lax.fori_loop(1, sp, greet, 0)
-    pl.semaphore_wait(barrier, tp - 1 + sp - 1)
-
-    def part(slot, c):
-        return tok.at[slot, :, pl.ds(c * span, span)]
+    pl.semaphore_signal(barrier, inc=1, device_id={"sp": side}, device_id_type=MESH)
+    signal_line(barrier, barrier)
+    pl.semaphore_wait(barrier, tp + has_left + has_right)
 
     def send(slot, c, target, s_sem, r_sem):
+        part = tok.at[slot, :, pl.ds(c * span, span)]
         return pltpu.make_async_remote_copy(
-            src_ref=part(slot, c), dst_ref=part(slot, c), send_sem=s_sem, recv_sem=r_sem,
+            src_ref=part, dst_ref=part, send_sem=s_sem, recv_sem=r_sem,
             device_id={"tp": target}, device_id_type=MESH,
+        )
+
+    def send_whole(slot):
+        return pltpu.make_async_remote_copy(
+            src_ref=tok.at[slot], dst_ref=tok.at[slot], send_sem=tsend.at[0, 0], recv_sem=trecv.at[0, 0],
+            device_id={"tp": partner}, device_id_type=MESH,
         )
 
     def peer(g):
@@ -96,65 +111,116 @@
 
     tok_load.wait()
     first_sends, forwards = [], []
+    cp = send_whole(me_tp)
+    cp.start()
+    first_sends.append(cp)
     for c in range(CHUNKS):
         for g in range(1, groups):
             cp = send(me_tp, c, peer(g), tsend.at[g, c], trecv.at[g, c])
             cp.start()
             first_sends.append(cp)
-        cp = send(me_tp, c, partner, tsend.at[0, c], trecv.at[0, c])
-        cp.start()
-        first_sends.append(cp)
 
     cosine, sine = rotary_tables(me_sp * rows, rows)
     tables[0] = cosine
     tables[1] = sine
+
+    def pass_on(_, carry):
+        signal_line(ready.at[0], ready.at[1])
+
+        @pl.when(me_z > 0)
+        def _():
+            pl.semaphore_wait(ready.at[0], 1)
+
+        @pl.when(me_z < depth_z - 1)
+        def _():
+            pl.semaphore_wait(ready.at[1], 1)
+
+        return carry
+
+    if depth_z > 2:
+        lax.fori_loop(0, depth_z - 2, pass_on, 0)
     for c in loads:
         c.wait()
 
-    acc_qk = jnp.zeros((rows, 4 * HEAD), jnp.float32)
-    acc_v = jnp.zeros((rows, 2 * HEAD), jnp.float32)
-    for c in range(CHUNKS):
-        for g in range(1, groups):
-            slot = lax.rem(me_tp + tp - 2 * g, tp)
+    me_chip = me_tp // 2
+    pair = 2 * own_rows
+
+    def kv_copy(slot, chip, order, i, device):
+        return pltpu.make_async_remote_copy(
+            src_ref=kv.at[slot, chip], dst_ref=kv.at[slot, chip],
+            send_sem=ksend.at[order, i], recv_sem=krecv.at[order, i],
+            device_id={"sp": device}, device_id_type=MESH,
+        )
+
+    upper = (2 * me_z) // depth_z
+
+    def distance(k):
+        return upper * k + (1 - upper) * (depth_z - k)
+
+    def along(d):
+        return 2 * lax.rem(me_z + d, depth_z) + me_sp % 2
+
+    def from_along(d):
+        return 2 * lax.rem(me_z + depth_z - d, depth_z) + me_sp % 2
+
+    def loop(count, body, state):
+        if count <= 8:
+            for k in range(1, count):
+                state = body(k, state)
+            return state
+        return lax.fori_loop(1, count, body, state)
+
+    def finish(chip, order, qk, values):
+        cosine = tables[0, pl.ds(pl.multiple_of(chip * pair, pair), pair), :]
+        sine = tables[1, pl.ds(pl.multiple_of(chip * pair, pair), pair), :]
+        kv[me_sp, chip, :, : 2 * HEAD] = turn(qk[:, 2 * HEAD :], cosine, sine).astype(jnp.bfloat16)
+        kv[me_sp, chip, :, 2 * HEAD :] = values.astype(jnp.bfloat16)
+
+        def start(k, carry):
+            d = distance(k)
+            kv_copy(me_sp, chip, order, d, along(d)).start()
+            return carry
+
+        kv_copy(me_sp, chip, order, 0, side).start()
+        loop(depth_z, start, 0)
+        queries = turn(qk[:, : 2 * HEAD], cosine, sine)
+        lane = lax.broadcasted_iota(jnp.int32, queries.shape, 1)
+        qbuf[0, pl.ds(pl.multiple_of(chip * pair, pair), pair), :] = jnp.where(lane < HEAD, queries, 0.0).astype(jnp.bfloat16)
+        qbuf[1, pl.ds(pl.multiple_of(chip * pair, pair), pair), :] = jnp.where(lane < HEAD, 0.0, queries).astype(jnp.bfloat16)
+
+    def project(base, lower, size):
+        x = tok[pl.ds(base, 2), :, lower : lower + size].reshape(pair, size)
+        return (
+            lax.dot_general(x, wqk[:, lower : lower + size], NT, preferred_element_type=jnp.float32),
+            jnp.dot(x, wvv[lower : lower + size, :], preferred_element_type=jnp.float32),
+        )
+
+    send_whole(partner).wait_recv()
+    finish(me_chip, 0, *project(2 * me_chip, 0, depth))
+    for g in range(1, groups):
+        chip = lax.rem(me_chip + groups - g, groups)
+        slot = 2 * chip + me_tp % 2
+        other = 2 * chip + partner % 2
+        qk = jnp.zeros((pair, 4 * HEAD), jnp.float32)
+        values = jnp.zeros((pair, 2 * HEAD), jnp.float32)
+        for c in range(CHUNKS):
             send(slot, c, partner, tsend.at[g, c], trecv.at[g, c]).wait_recv()
             cp = send(slot, c, partner, fsend.at[g, c], frecv.at[g, c])
             cp.start()
             forwards.append(cp)
-        send(partner, c, partner, tsend.at[0, c], trecv.at[0, c]).wait_recv()
-        for g in range(1, groups):
-            slot = lax.rem(partner + tp - 2 * g, tp)
-            send(slot, c, partner, fsend.at[g, c], frecv.at[g, c]).wait_recv()
-        x = tok[:, :, c * span:(c + 1) * span].reshape(rows, span)
-        acc_qk += lax.dot_general(x, wqk[:, c * span:(c + 1) * span], NT, preferred_element_type=jnp.float32)
-        acc_v += jnp.dot(x, wvv[c * span:(c + 1) * span, :], preferred_element_type=jnp.float32)
-
-    cosine, sine = tables[0], tables[1]
-    keys = turn(acc_qk[:, 2 * HEAD:], cosine, sine).astype(jnp.bfloat16)
-    kv[me_sp, :, : 2 * HEAD] = keys
-    kv[me_sp, :, 2 * HEAD :] = acc_v.astype(jnp.bfloat16)
-
-    def kv_copy(slot, d, target):
-        return pltpu.make_async_remote_copy(
-            src_ref=kv.at[slot], dst_ref=kv.at[slot], send_sem=ksend.at[d], recv_sem=krecv.at[d],
-            device_id={"sp": target}, device_id_type=MESH,
-        )
-
-    def start_kv(d, _):
-        kv_copy(me_sp, d, lax.rem(me_sp + d, sp)).start()
-        return _
-
-    lax.fori_loop(1, sp, start_kv, 0)
-
-    queries = turn(acc_qk[:, : 2 * HEAD], cosine, sine)
-    lane = lax.broadcasted_iota(jnp.int32, queries.shape, 1)
-    both = jnp.concatenate(
-        [jnp.where(lane < HEAD, queries, 0.0), jnp.where(lane < HEAD, 0.0, queries)], axis=0
-    ).astype(jnp.bfloat16)
-
-    def absorb(slot, state):
+            send(other, c, partner, fsend.at[g, c], frecv.at[g, c]).wait_recv()
+            more = project(2 * chip, c * span, span)
+            qk += more[0]
+            values += more[1]
+        finish(chip, g, qk, values)
+
+    both = qbuf[...].reshape(2 * rows, 2 * HEAD)
+
+    def absorb(blocks, state):
         peak, total, summed = state
-        k = kv[slot, :, : 2 * HEAD]
-        v = kv[slot, :, 2 * HEAD :]
+        block = jnp.concatenate([kv[slot, chip] for slot, chip in blocks], axis=0)
+        k = block[:, : 2 * HEAD]
+        v = block[:, 2 * HEAD :]
         scores = lax.dot_general(both, k, NT, preferred_element_type=jnp.float32) * HEAD ** (-0.5)
         new_peak = jnp.maximum(peak, jnp.max(scores, axis=1, keepdims=True))
         factor = jnp.exp(peak - new_peak)
@@ -165,23 +231,58 @@
         )
         return new_peak, total, summed
 
+    def absorb_line(sources, chip, also, state):
+        if depth_z <= 8:
+            return absorb([(sources(distance(k)), chip) for k in range(1, depth_z)] + also, state)
+        if also:
+            state = absorb(also, state)
+        return lax.fori_loop(1, depth_z, lambda k, s: absorb([(sources(distance(k)), chip)], s), state)
+
+    def side_of(d):
+        slot = from_along(d)
+        return slot + 1 - 2 * (slot % 2)
+
     state = (
         jnp.full((2 * rows, 1), floor_value, jnp.float32),
         jnp.zeros((2 * rows, 1), jnp.float32),
         jnp.zeros((2 * rows, 2 * HEAD), jnp.float32),
     )
-    state = absorb(me_sp, state)
-
-    def step(d, state):
-        slot = lax.rem(me_sp + sp - d, sp)
-        kv_copy(slot, d, slot).wait_recv()
-        return absorb(slot, state)
-
-    if sp <= 16:
-        for d in range(1, sp):
-            state = step(d, state)
-    else:
-        state = lax.fori_loop(1, sp, step, state)
+    state = absorb([(me_sp, h) for h in range(groups)], state)
+
+    def chip_of(order):
+        return lax.rem(me_chip + groups - order, groups)
+
+    def relay(order):
+        chip = chip_of(order)
+
+        def one(k, carry):
+            d = distance(k)
+            kv_copy(from_along(d), chip, order, d, side).wait_recv()
+            kv_copy(from_along(d), chip, order, depth_z + d, side).start()
+            return carry
+
+        loop(depth_z, one, 0)
+
+    def relayed(order):
+        chip = chip_of(order)
+
+        def one(k, carry):
+            d = distance(k)
+            kv_copy(side_of(d), chip, order, depth_z + d, side).wait_recv()
+            return carry
+
+        loop(depth_z, one, 0)
+
+    for order in range(groups):
+        chip = chip_of(order)
+        relay(order)
+        if order > 0:
+            relayed(order - 1)
+            state = absorb_line(side_of, chip_of(order - 1), [], state)
+        kv_copy(side, chip, order, 0, side).wait_recv()
+        state = absorb_line(from_along, chip, [(side, chip)], state)
+    relayed(groups - 1)
+    state = absorb_line(side_of, chip_of(groups - 1), [], state)
 
     _, total, summed = state
     ratio = summed / total
@@ -210,11 +311,14 @@
     for cp in first_sends + forwards + head_sends:
         cp.wait_send()
 
-    def drain(d, _):
-        kv_copy(me_sp, d, lax.rem(me_sp + d, sp)).wait_send()
-        return _
-
-    lax.fori_loop(1, sp, drain, 0)
+    for order in range(groups):
+
+        def drain(i, carry):
+            kv_copy(me_sp, 0, order, i, side).wait_send()
+            return carry
+
+        lax.fori_loop(0, depth_z, drain, 0)
+        lax.fori_loop(depth_z + 1, 2 * depth_z, drain, 0)
 
 
 def per_device(
@@ -239,7 +343,8 @@
             pltpu.VMEM((depth, 2 * HEAD), bf16),
             pltpu.VMEM(out_weight.shape, bf16),
             pltpu.VMEM((2, rows, 2 * HEAD), jnp.float32),
-            pltpu.VMEM((sp, rows, 4 * HEAD), bf16),
+            pltpu.VMEM((sp, tp // 2, 2 * own_rows, 4 * HEAD), bf16),
+            pltpu.VMEM((2, rows, 2 * HEAD), bf16),
             pltpu.VMEM((tp, own_rows, 2 * HEAD), bf16),
             pltpu.VMEM((tp, own_rows, 2 * HEAD), bf16),
             dma((7,)),
@@ -247,10 +352,11 @@
             dma((tp // 2, CHUNKS)),
             dma((tp // 2, CHUNKS)),
             dma((tp // 2, CHUNKS)),
-            dma((sp,)),
-            dma((sp,)),
+            dma((tp // 2, sp)),
+            dma((tp // 2, sp)),
             dma((tp,)),
             dma((tp,)),
+            pltpu.SemaphoreType.REGULAR((2,)),
         ],
         compiler_params=pltpu.CompilerParams(
             collective_id=0, has_side_effects=True, vmem_limit_bytes=56 * 1024 * 1024

time: 32.7 us -> 28.8 us (0.88)
  Pallas kernels: 30.3 us -> 26.4 us
    pallas_call x1, Pallas kernels: 30.3 us -> 26.4 us  [per_device(): pl.pallas_call(functools.partial(kernel, sp, tp), out_shape=jax.ShapeDtyp...]
where the time goes in v2:
time: 28.8 us; the launch traced here: 28.6 us
  Pallas kernels  26.4 us (92%)
  local copies, waits for them, and re-layouts  1.57 us (5%)
  between operations  0.66 us (2%)
    pallas_call x1, Pallas kernels, per_device(): pl.pallas_call(functools.partial(kernel, sp, tp), out_shape=jax.ShapeDtyp...  26.4 us
    unnamed x1, local copies, waits for them, and re-layouts  1.57 us

profile of v2, /device:TPU:0, one launch (start us, length us, event | category | flops | bytes accessed | tf_op | source)
XLA Modules:
  0.0 28.6 jit_solution(17014758971535634385)
XLA Ops:
  0.7 26.4 %shard_map.91 = bf16[32,2048]{1,0:T(8,128)(2,1)} custom-call(bf16[32,2048]{1,0:T(8,128)(2,1)} %tokens.1, bf16[64,2048]{1,0:T(8,128)(2,1)} %bitcast.5, bf16[64,2048]{1,0:T(8,128)(2,1)} %bitcast.6, bf16[64,2048]{1,0:T(8,128)(2,1)} %bitcast.7, bf16[64,2048]{1,0:T(8,128)(2,1)} %bitcast.8, bf16[2048,128]{1,0:T(8,128)(2,1)} %wv.1, f32[1]{0:T(128)S(6)} %copy.11.mixing, ...), custom_call_target="tpu_custom_call" | custom-call | tf_op jit(solution)/shard_map/pallas_call | solution.py:335
  27.1 1.6 %copy.12 = bf16[32,2048]{1,0:T(8,128)(2,1)} copy(bf16[32,2048]{1,0:T(8,128)(2,1)} %shard_map.91) | data formatting | bytes 262144

commit v3 on v2

--- a/solution.py
+++ b/solution.py
@@ -50,7 +50,7 @@
     sp, tp,
     tokens, wq1, wq2, wk1, wk2, wv, mixing, wo, gain, out,
     tok, wqk, wvv, wov, tables, kv, qbuf, hsend, hrecv,
-    load_sems, tsend, trecv, fsend, frecv, ksend, krecv, hs_sems, hr_sems, ready,
+    load_sems, tsend, trecv, fsend, frecv, ksend, krecv, hs_sems, hr_sems, ready, mix_in, gain_in,
 ):
     own_rows, depth = tokens.shape
     rows = own_rows * tp
@@ -60,6 +60,26 @@
     partner = me_tp + 1 - 2 * (me_tp % 2)
     span = depth // CHUNKS
 
+    depth_z = sp // 2
+    me_z = me_sp // 2
+    side = me_sp + 1 - 2 * (me_sp % 2)
+    barrier = pltpu.get_barrier_semaphore()
+    has_left = jnp.minimum(me_z, 1)
+    has_right = jnp.minimum(depth_z - 1 - me_z, 1)
+
+    def signal_line(left_sem, right_sem):
+        @pl.when(me_z > 0)
+        def _():
+            pl.semaphore_signal(right_sem, inc=1, device_id={"sp": me_sp - 2}, device_id_type=MESH)
+
+        @pl.when(me_z < depth_z - 1)
+        def _():
+            pl.semaphore_signal(left_sem, inc=1, device_id={"sp": me_sp + 2}, device_id_type=MESH)
+
+    for d in range(1, tp):
+        pl.semaphore_signal(barrier, inc=1, device_id={"tp": lax.rem(me_tp + d, tp)}, device_id_type=MESH)
+    pl.semaphore_signal(barrier, inc=1, device_id={"sp": side}, device_id_type=MESH)
+    signal_line(barrier, barrier)
     tok_load = pltpu.make_async_copy(tokens, tok.at[me_tp], load_sems.at[0])
     tok_load.start()
     loads = []
@@ -70,27 +90,13 @@
         c.start()
     wo_load = pltpu.make_async_copy(wo, wov, load_sems.at[6])
     wo_load.start()
-
-    depth_z = sp // 2
-    me_z = me_sp // 2
-    side = me_sp + 1 - 2 * (me_sp % 2)
-    barrier = pltpu.get_barrier_semaphore()
-    has_left = jnp.minimum(me_z, 1)
-    has_right = jnp.minimum(depth_z - 1 - me_z, 1)
-
-    def signal_line(left_sem, right_sem):
-        @pl.when(me_z > 0)
-        def _():
-            pl.semaphore_signal(right_sem, inc=1, device_id={"sp": me_sp - 2}, device_id_type=MESH)
-
-        @pl.when(me_z < depth_z - 1)
-        def _():
-            pl.semaphore_signal(left_sem, inc=1, device_id={"sp": me_sp + 2}, device_id_type=MESH)
-
-    for d in range(1, tp):
-        pl.semaphore_signal(barrier, inc=1, device_id={"tp": lax.rem(me_tp + d, tp)}, device_id_type=MESH)
-    pl.semaphore_signal(barrier, inc=1, device_id={"sp": side}, device_id_type=MESH)
-    signal_line(barrier, barrier)
+    small = [
+        pltpu.make_async_copy(mixing, mix_in, load_sems.at[7]),
+        pltpu.make_async_copy(gain, gain_in, load_sems.at[8]),
+    ]
+    for c in small:
+        c.start()
+
     pl.semaphore_wait(barrier, tp + has_left + has_right)
 
     def send(slot, c, target, s_sem, r_sem):
@@ -139,7 +145,7 @@
 
     if depth_z > 2:
         lax.fori_loop(0, depth_z - 2, pass_on, 0)
-    for c in loads:
+    for c in loads + small + [wo_load]:
         c.wait()
 
     me_chip = me_tp // 2
@@ -286,9 +292,9 @@
 
     _, total, summed = state
     ratio = summed / total
-    mixed = ratio[:rows] - mixing[0] * ratio[rows:]
+    mixed = ratio[:rows] - mix_in[...] * ratio[rows:]
     normed = (
-        mixed * lax.rsqrt(jnp.mean(mixed * mixed, axis=-1, keepdims=True) + epsilon) * gain[...]
+        mixed * lax.rsqrt(jnp.mean(mixed * mixed, axis=-1, keepdims=True) + epsilon) * gain_in[...]
     )
     hsend[...] = normed.astype(jnp.bfloat16).reshape(tp, own_rows, 2 * HEAD)
     head_sends = []
@@ -302,7 +308,6 @@
         cp.start()
         head_sends.append(cp)
     hrecv[me_tp] = hsend[me_tp]
-    wo_load.wait()
     for cp in head_sends:
         cp.wait_recv()
     joined = jnp.concatenate([hrecv[h] for h in range(tp)], axis=1)
@@ -334,8 +339,8 @@
     bf16 = jnp.bfloat16
     return pl.pallas_call(
         functools.partial(kernel, sp, tp),
-        out_shape=jax.ShapeDtypeStruct((own_rows, out_weight.shape[1]), bf16),
-        in_specs=[any_spec] * 6 + [pl.BlockSpec(memory_space=pltpu.SMEM), any_spec, vmem],
+        out_shape=pltpu.VMEM((own_rows, out_weight.shape[1]), bf16),
+        in_specs=[any_spec] * 6 + [any_spec] * 3,
         out_specs=vmem,
         scratch_shapes=[
             pltpu.VMEM((tp, own_rows, depth), bf16),
@@ -347,7 +352,7 @@
             pltpu.VMEM((2, rows, 2 * HEAD), bf16),
             pltpu.VMEM((tp, own_rows, 2 * HEAD), bf16),
             pltpu.VMEM((tp, own_rows, 2 * HEAD), bf16),
-            dma((7,)),
+            dma((9,)),
             dma((tp // 2, CHUNKS)),
             dma((tp // 2, CHUNKS)),
             dma((tp // 2, CHUNKS)),
@@ -357,13 +362,15 @@
             dma((tp,)),
             dma((tp,)),
             pltpu.SemaphoreType.REGULAR((2,)),
+            pltpu.VMEM((1, 1), jnp.float32),
+            pltpu.VMEM((1, 2 * HEAD), jnp.float32),
         ],
         compiler_params=pltpu.CompilerParams(
             collective_id=0, has_side_effects=True, vmem_limit_bytes=56 * 1024 * 1024
         ),
     )(
         tokens, query_one.T, query_two.T, key_one.T, key_two.T, value_weight,
-        mixing, out_weight, head_gain.reshape(1, -1),
+        mixing.reshape(1, 1), out_weight, head_gain.reshape(1, -1),
     )
 
 

time: 28.8 us -> 26.6 us (0.924)
  Pallas kernels: 26.4 us -> 25.1 us
  local copies, waits for them, and re-layouts: 1.57 us -> 0.66 us
    pallas_call x1, Pallas kernels: 26.4 us -> 25.1 us  [per_device(): pl.pallas_call(functools.partial(kernel, sp, tp), out_shape=pltpu.VMEM((o...]
    unnamed x1, local copies, waits for them, and re-layouts: 1.57 us -> 0.66 us
where the time goes in v3:
time: 26.6 us; the launch traced here: 26.5 us
  Pallas kernels  25.1 us (94%)
  local copies, waits for them, and re-layouts  0.66 us (2%)
  between operations  0.66 us (2%)
    pallas_call x1, Pallas kernels, per_device(): pl.pallas_call(functools.partial(kernel, sp, tp), out_shape=pltpu.VMEM((o...  25.1 us
    unnamed x1, local copies, waits for them, and re-layouts  0.66 us

profile of v3, /device:TPU:0, one launch (start us, length us, event | category | flops | bytes accessed | tf_op | source)
XLA Modules:
  0.0 26.5 jit_solution(2647314477410035323)
XLA Ops:
  0.7 25.1 %shard_map.91 = bf16[32,2048]{1,0:T(8,128)(2,1)S(1)} custom-call(bf16[32,2048]{1,0:T(8,128)(2,1)} %tokens.1, bf16[64,2048]{1,0:T(8,128)(2,1)} %bitcast.7, bf16[64,2048]{1,0:T(8,128)(2,1)} %bitcast.8, bf16[64,2048]{1,0:T(8,128)(2,1)} %bitcast.9, bf16[64,2048]{1,0:T(8,128)(2,1)} %bitcast.10, bf16[2048,128]{1,0:T(8,128)(2,1)} %wv.1, f32[1,1]{1,0:T(1,128)} %bitcast.6.mixing, ...), custom_call_target="tpu_custom_call" | custom-call | tf_op jit(solution)/shard_map/pallas_call | solution.py:340
  25.8 0.7 %copy.11 = bf16[32,2048]{1,0:T(8,128)(2,1)} copy(bf16[32,2048]{1,0:T(8,128)(2,1)S(1)} %shard_map.91) | data formatting | bytes 262144

commit v4 on v3

--- a/solution.py
+++ b/solution.py
@@ -17,13 +17,17 @@
 floor_value = -1e30
 MESH = pl.DeviceIdType.MESH
 NT = (((1,), (1,)), ((), ()))
-CHUNKS = 4
-
-
-def rotary_tables(start, rows):
+PIECES = 2
+
+
+def rotary_tables(start, rows, own_rows):
     shape = (rows, 2 * HEAD)
     lane = lax.broadcasted_iota(jnp.int32, shape, 1)
-    token = lax.broadcasted_iota(jnp.int32, shape, 0) + start
+    index = lax.broadcasted_iota(jnp.int32, shape, 0)
+    half = own_rows // PIECES
+    device = 2 * (index // (2 * own_rows)) + (index % own_rows) // half
+    piece = (index % (2 * own_rows)) // own_rows
+    token = start + device * own_rows + piece * half + index % half
     entry = lane % QUARTER
     freqs = jnp.zeros(shape, jnp.float32)
     for j in range(QUARTER):
@@ -58,7 +62,10 @@
     me_tp = lax.axis_index("tp")
     me_sp = lax.axis_index("sp")
     partner = me_tp + 1 - 2 * (me_tp % 2)
-    span = depth // CHUNKS
+    half = own_rows // PIECES
+    pair = 2 * own_rows
+    me_chip = me_tp // 2
+    orders = [(0, None)] + [(g, r) for g in range(1, groups) for r in range(PIECES)]
 
     depth_z = sp // 2
     me_z = me_sp // 2
@@ -100,7 +107,7 @@
     pl.semaphore_wait(barrier, tp + has_left + has_right)
 
     def send(slot, c, target, s_sem, r_sem):
-        part = tok.at[slot, :, pl.ds(c * span, span)]
+        part = tok.at[slot, pl.ds(c * half, half)]
         return pltpu.make_async_remote_copy(
             src_ref=part, dst_ref=part, send_sem=s_sem, recv_sem=r_sem,
             device_id={"tp": target}, device_id_type=MESH,
@@ -120,13 +127,13 @@
     cp = send_whole(me_tp)
     cp.start()
     first_sends.append(cp)
-    for c in range(CHUNKS):
+    for c in range(PIECES):
         for g in range(1, groups):
             cp = send(me_tp, c, peer(g), tsend.at[g, c], trecv.at[g, c])
             cp.start()
             first_sends.append(cp)
 
-    cosine, sine = rotary_tables(me_sp * rows, rows)
+    cosine, sine = rotary_tables(me_sp * rows, rows, own_rows)
     tables[0] = cosine
     tables[1] = sine
 
@@ -148,12 +155,18 @@
     for c in loads + small + [wo_load]:
         c.wait()
 
-    me_chip = me_tp // 2
-    pair = 2 * own_rows
-
-    def kv_copy(slot, chip, order, i, device):
+    def chip_of(order):
+        return lax.rem(me_chip + groups - orders[order][0], groups)
+
+    def held(slot, order):
+        piece = orders[order][1]
+        if piece is None:
+            return kv.at[slot, chip_of(order)]
+        return kv.at[slot, chip_of(order), piece]
+
+    def kv_copy(slot, order, i, device):
         return pltpu.make_async_remote_copy(
-            src_ref=kv.at[slot, chip], dst_ref=kv.at[slot, chip],
+            src_ref=held(slot, order), dst_ref=held(slot, order),
             send_sem=ksend.at[order, i], recv_sem=krecv.at[order, i],
             device_id={"sp": device}, device_id_type=MESH,
         )
@@ -176,55 +189,60 @@
             return state
         return lax.fori_loop(1, count, body, state)
 
-    def finish(chip, order, qk, values):
-        cosine = tables[0, pl.ds(pl.multiple_of(chip * pair, pair), pair), :]
-        sine = tables[1, pl.ds(pl.multiple_of(chip * pair, pair), pair), :]
-        kv[me_sp, chip, :, : 2 * HEAD] = turn(qk[:, 2 * HEAD :], cosine, sine).astype(jnp.bfloat16)
-        kv[me_sp, chip, :, 2 * HEAD :] = values.astype(jnp.bfloat16)
-
-        def start(k, carry):
+    def finish(order):
+        chip = chip_of(order)
+        piece = orders[order][1]
+        pieces = range(PIECES) if piece is None else (piece,)
+        x = jnp.concatenate(
+            [
+                tok[pl.ds(2 * chip, 2), r * half : (r + 1) * half, :].reshape(own_rows, depth)
+                for r in pieces
+            ],
+            axis=0,
+        )
+        count = x.shape[0]
+        qk = lax.dot_general(x, wqk[...], NT, preferred_element_type=jnp.float32)
+        values = jnp.dot(x, wvv[...], preferred_element_type=jnp.float32)
+        start = pl.multiple_of(chip * pair + pieces[0] * own_rows, own_rows)
+        where = pl.ds(start, count)
+        cosine = tables[0, where, :]
+        sine = tables[1, where, :]
+        keys = turn(qk[:, 2 * HEAD :], cosine, sine).astype(jnp.bfloat16)
+        values = values.astype(jnp.bfloat16)
+        for i, r in enumerate(pieces):
+            kv[me_sp, chip, r, :, : 2 * HEAD] = keys[i * own_rows : (i + 1) * own_rows]
+            kv[me_sp, chip, r, :, 2 * HEAD :] = values[i * own_rows : (i + 1) * own_rows]
+
+        def start_line(k, carry):
             d = distance(k)
-            kv_copy(me_sp, chip, order, d, along(d)).start()
+            kv_copy(me_sp, order, d, along(d)).start()
             return carry
 
-        kv_copy(me_sp, chip, order, 0, side).start()
-        loop(depth_z, start, 0)
+        loop(depth_z, start_line, 0)
+        kv_copy(me_sp, order, 0, side).start()
         queries = turn(qk[:, : 2 * HEAD], cosine, sine)
         lane = lax.broadcasted_iota(jnp.int32, queries.shape, 1)
-        qbuf[0, pl.ds(pl.multiple_of(chip * pair, pair), pair), :] = jnp.where(lane < HEAD, queries, 0.0).astype(jnp.bfloat16)
-        qbuf[1, pl.ds(pl.multiple_of(chip * pair, pair), pair), :] = jnp.where(lane < HEAD, 0.0, queries).astype(jnp.bfloat16)
-
-    def project(base, lower, size):
-        x = tok[pl.ds(base, 2), :, lower : lower + size].reshape(pair, size)
-        return (
-            lax.dot_general(x, wqk[:, lower : lower + size], NT, preferred_element_type=jnp.float32),
-            jnp.dot(x, wvv[lower : lower + size, :], preferred_element_type=jnp.float32),
-        )
+        qbuf[0, where, :] = jnp.where(lane < HEAD, queries, 0.0).astype(jnp.bfloat16)
+        qbuf[1, where, :] = jnp.where(lane < HEAD, 0.0, queries).astype(jnp.bfloat16)
 
     send_whole(partner).wait_recv()
-    finish(me_chip, 0, *project(2 * me_chip, 0, depth))
-    for g in range(1, groups):
-        chip = lax.rem(me_chip + groups - g, groups)
-        slot = 2 * chip + me_tp % 2
-        other = 2 * chip + partner % 2
-        qk = jnp.zeros((pair, 4 * HEAD), jnp.float32)
-        values = jnp.zeros((pair, 2 * HEAD), jnp.float32)
-        for c in range(CHUNKS):
-            send(slot, c, partner, tsend.at[g, c], trecv.at[g, c]).wait_recv()
-            cp = send(slot, c, partner, fsend.at[g, c], frecv.at[g, c])
-            cp.start()
-            forwards.append(cp)
-            send(other, c, partner, fsend.at[g, c], frecv.at[g, c]).wait_recv()
-            more = project(2 * chip, c * span, span)
-            qk += more[0]
-            values += more[1]
-        finish(chip, g, qk, values)
+    finish(0)
+    for order in range(1, len(orders)):
+        g, r = orders[order]
+        slot = 2 * chip_of(order) + me_tp % 2
+        other = 2 * chip_of(order) + partner % 2
+        send(slot, r, partner, tsend.at[g, r], trecv.at[g, r]).wait_recv()
+        cp = send(slot, r, partner, fsend.at[g, r], frecv.at[g, r])
+        cp.start()
+        forwards.append(cp)
+        send(other, r, partner, fsend.at[g, r], frecv.at[g, r]).wait_recv()
+        finish(order)
 
     both = qbuf[...].reshape(2 * rows, 2 * HEAD)
 
     def absorb(blocks, state):
         peak, total, summed = state
-        block = jnp.concatenate([kv[slot, chip] for slot, chip in blocks], axis=0)
+        block = jnp.concatenate([b[...].reshape(-1, 4 * HEAD) for b in blocks], axis=0)
         k = block[:, : 2 * HEAD]
         v = block[:, 2 * HEAD :]
         scores = lax.dot_general(both, k, NT, preferred_element_type=jnp.float32) * HEAD ** (-0.5)
@@ -237,12 +255,15 @@
         )
         return new_peak, total, summed
 
-    def absorb_line(sources, chip, also, state):
+    def absorb_line(sources, order, also, state):
         if depth_z <= 8:
-            return absorb([(sources(distance(k)), chip) for k in range(1, depth_z)] + also, state)
+            line = [held(sources(distance(k)), order) for k in range(1, depth_z)]
+            return absorb(line + also, state)
         if also:
             state = absorb(also, state)
-        return lax.fori_loop(1, depth_z, lambda k, s: absorb([(sources(distance(k)), chip)], s), state)
+        return lax.fori_loop(
+            1, depth_z, lambda k, s: absorb([held(sources(distance(k)), order)], s), state
+        )
 
     def side_of(d):
         slot = from_along(d)
@@ -253,42 +274,34 @@
         jnp.zeros((2 * rows, 1), jnp.float32),
         jnp.zeros((2 * rows, 2 * HEAD), jnp.float32),
     )
-    state = absorb([(me_sp, h) for h in range(groups)], state)
-
-    def chip_of(order):
-        return lax.rem(me_chip + groups - order, groups)
+    state = absorb([kv.at[me_sp]], state)
 
     def relay(order):
-        chip = chip_of(order)
-
         def one(k, carry):
             d = distance(k)
-            kv_copy(from_along(d), chip, order, d, side).wait_recv()
-            kv_copy(from_along(d), chip, order, depth_z + d, side).start()
+            kv_copy(from_along(d), order, d, side).wait_recv()
+            kv_copy(from_along(d), order, depth_z + d, side).start()
             return carry
 
         loop(depth_z, one, 0)
 
-    def relayed(order):
-        chip = chip_of(order)
-
+    def relayed(order, state):
         def one(k, carry):
             d = distance(k)
-            kv_copy(side_of(d), chip, order, depth_z + d, side).wait_recv()
+            kv_copy(side_of(d), order, depth_z + d, side).wait_recv()
             return carry
 
         loop(depth_z, one, 0)
-
-    for order in range(groups):
-        chip = chip_of(order)
+        return absorb_line(side_of, order, [], state)
+
+    last = len(orders) - 1
+    for order in range(last + 1):
         relay(order)
         if order > 0:
-            relayed(order - 1)
-            state = absorb_line(side_of, chip_of(order - 1), [], state)
-        kv_copy(side, chip, order, 0, side).wait_recv()
-        state = absorb_line(from_along, chip, [(side, chip)], state)
-    relayed(groups - 1)
-    state = absorb_line(side_of, chip_of(groups - 1), [], state)
+            state = relayed(order - 1, state)
+        kv_copy(side, order, 0, side).wait_recv()
+        state = absorb_line(from_along, order, [held(side, order)], state)
+    state = relayed(last, state)
 
     _, total, summed = state
     ratio = summed / total
@@ -296,7 +309,10 @@
     normed = (
         mixed * lax.rsqrt(jnp.mean(mixed * mixed, axis=-1, keepdims=True) + epsilon) * gain_in[...]
     )
-    hsend[...] = normed.astype(jnp.bfloat16).reshape(tp, own_rows, 2 * HEAD)
+    heads = normed.astype(jnp.bfloat16).reshape(groups, PIECES, 2, half, 2 * HEAD)
+    for device in range(tp):
+        for r in range(PIECES):
+            hsend[device, r * half : (r + 1) * half, :] = heads[device // 2, r, device % 2]
     head_sends = []
     for d in range(1, tp):
         target = lax.rem(me_tp + d, tp)
@@ -316,10 +332,10 @@
     for cp in first_sends + forwards + head_sends:
         cp.wait_send()
 
-    for order in range(groups):
+    for order in range(last + 1):
 
         def drain(i, carry):
-            kv_copy(me_sp, 0, order, i, side).wait_send()
+            kv_copy(me_sp, order, i, side).wait_send()
             return carry
 
         lax.fori_loop(0, depth_z, drain, 0)
@@ -348,17 +364,17 @@
             pltpu.VMEM((depth, 2 * HEAD), bf16),
             pltpu.VMEM(out_weight.shape, bf16),
             pltpu.VMEM((2, rows, 2 * HEAD), jnp.float32),
-            pltpu.VMEM((sp, tp // 2, 2 * own_rows, 4 * HEAD), bf16),
+            pltpu.VMEM((sp, tp // 2, PIECES, own_rows, 4 * HEAD), bf16),
             pltpu.VMEM((2, rows, 2 * HEAD), bf16),
             pltpu.VMEM((tp, own_rows, 2 * HEAD), bf16),
             pltpu.VMEM((tp, own_rows, 2 * HEAD), bf16),
             dma((9,)),
-            dma((tp // 2, CHUNKS)),
-            dma((tp // 2, CHUNKS)),
-            dma((tp // 2, CHUNKS)),
-            dma((tp // 2, CHUNKS)),
-            dma((tp // 2, sp)),
-            dma((tp // 2, sp)),
+            dma((tp // 2, PIECES)),
+            dma((tp // 2, PIECES)),
+            dma((tp // 2, PIECES)),
+            dma((tp // 2, PIECES)),
+            dma((1 + PIECES * (tp // 2 - 1), sp)),
+            dma((1 + PIECES * (tp // 2 - 1), sp)),
             dma((tp,)),
             dma((tp,)),
             pltpu.SemaphoreType.REGULAR((2,)),

time: 26.6 us -> 25.7 us (0.966)
  Pallas kernels: 25.1 us -> 24.3 us
    pallas_call x1, Pallas kernels: 25.1 us -> 24.3 us  [per_device(): pl.pallas_call(functools.partial(kernel, sp, tp), out_shape=pltpu.VMEM((o...]
where the time goes in v4:
time: 25.7 us; the launch traced here: 25.6 us
  Pallas kernels  24.3 us (95%)
  local copies, waits for them, and re-layouts  0.66 us (3%)
  between operations  0.66 us (3%)
    pallas_call x1, Pallas kernels, per_device(): pl.pallas_call(functools.partial(kernel, sp, tp), out_shape=pltpu.VMEM((o...  24.3 us
    unnamed x1, local copies, waits for them, and re-layouts  0.66 us

profile of v4, /device:TPU:0, one launch (start us, length us, event | category | flops | bytes accessed | tf_op | source)
XLA Modules:
  0.0 25.6 jit_solution(15537855768562542952)
XLA Ops:
  0.7 24.3 %shard_map.91 = bf16[32,2048]{1,0:T(8,128)(2,1)S(1)} custom-call(bf16[32,2048]{1,0:T(8,128)(2,1)} %tokens.1, bf16[64,2048]{1,0:T(8,128)(2,1)} %bitcast.7, bf16[64,2048]{1,0:T(8,128)(2,1)} %bitcast.8, bf16[64,2048]{1,0:T(8,128)(2,1)} %bitcast.9, bf16[64,2048]{1,0:T(8,128)(2,1)} %bitcast.10, bf16[2048,128]{1,0:T(8,128)(2,1)} %wv.1, f32[1,1]{1,0:T(1,128)} %bitcast.6.mixing, ...), custom_call_target="tpu_custom_call" | custom-call | tf_op jit(solution)/shard_map/pallas_call | solution.py:356
  24.9 0.7 %copy.11 = bf16[32,2048]{1,0:T(8,128)(2,1)} copy(bf16[32,2048]{1,0:T(8,128)(2,1)S(1)} %shard_map.91) | data formatting | bytes 262144

commit v5 on v4

--- a/solution.py
+++ b/solution.py
@@ -96,7 +96,6 @@
     for c in loads:
         c.start()
     wo_load = pltpu.make_async_copy(wo, wov, load_sems.at[6])
-    wo_load.start()
     small = [
         pltpu.make_async_copy(mixing, mix_in, load_sems.at[7]),
         pltpu.make_async_copy(gain, gain_in, load_sems.at[8]),
@@ -122,6 +121,8 @@
     def peer(g):
         return lax.rem(me_tp + 2 * g, tp)
 
+    if depth_z > 2:
+        signal_line(ready.at[0], ready.at[1])
     tok_load.wait()
     first_sends, forwards = [], []
     cp = send_whole(me_tp)
@@ -137,9 +138,7 @@
     tables[0] = cosine
     tables[1] = sine
 
-    def pass_on(_, carry):
-        signal_line(ready.at[0], ready.at[1])
-
+    def wait_line():
         @pl.when(me_z > 0)
         def _():
             pl.semaphore_wait(ready.at[0], 1)
@@ -148,12 +147,16 @@
         def _():
             pl.semaphore_wait(ready.at[1], 1)
 
+    def pass_on(_, carry):
+        wait_line()
+        signal_line(ready.at[0], ready.at[1])
         return carry
 
-    if depth_z > 2:
-        lax.fori_loop(0, depth_z - 2, pass_on, 0)
-    for c in loads + small + [wo_load]:
+    if depth_z > 3:
+        lax.fori_loop(0, depth_z - 3, pass_on, 0)
+    for c in loads + small:
         c.wait()
+    wo_load.start()
 
     def chip_of(order):
         return lax.rem(me_chip + groups - orders[order][0], groups)
@@ -213,6 +216,9 @@
             kv[me_sp, chip, r, :, : 2 * HEAD] = keys[i * own_rows : (i + 1) * own_rows]
             kv[me_sp, chip, r, :, 2 * HEAD :] = values[i * own_rows : (i + 1) * own_rows]
 
+        if order == 0 and depth_z > 2:
+            wait_line()
+
         def start_line(k, carry):
             d = distance(k)
             kv_copy(me_sp, order, d, along(d)).start()
@@ -324,6 +330,7 @@
         cp.start()
         head_sends.append(cp)
     hrecv[me_tp] = hsend[me_tp]
+    wo_load.wait()
     for cp in head_sends:
         cp.wait_recv()
     joined = jnp.concatenate([hrecv[h] for h in range(tp)], axis=1)

time: 25.7 us -> 24.9 us (0.969)
  Pallas kernels: 24.3 us -> 23.5 us
    pallas_call x1, Pallas kernels: 24.3 us -> 23.5 us  [per_device(): pl.pallas_call(functools.partial(kernel, sp, tp), out_shape=pltpu.VMEM((o...]
where the time goes in v5:
time: 24.9 us; the launch traced here: 24.8 us
  Pallas kernels  23.5 us (94%)
  local copies, waits for them, and re-layouts  0.66 us (3%)
  between operations  0.66 us (3%)
    pallas_call x1, Pallas kernels, per_device(): pl.pallas_call(functools.partial(kernel, sp, tp), out_shape=pltpu.VMEM((o...  23.5 us
    unnamed x1, local copies, waits for them, and re-layouts  0.66 us

profile of v5, /device:TPU:0, one launch (start us, length us, event | category | flops | bytes accessed | tf_op | source)
XLA Modules:
  0.0 24.8 jit_solution(18106504457100416937)
XLA Ops:
  0.7 23.5 %shard_map.91 = bf16[32,2048]{1,0:T(8,128)(2,1)S(1)} custom-call(bf16[32,2048]{1,0:T(8,128)(2,1)} %tokens.1, bf16[64,2048]{1,0:T(8,128)(2,1)} %bitcast.7, bf16[64,2048]{1,0:T(8,128)(2,1)} %bitcast.8, bf16[64,2048]{1,0:T(8,128)(2,1)} %bitcast.9, bf16[64,2048]{1,0:T(8,128)(2,1)} %bitcast.10, bf16[2048,128]{1,0:T(8,128)(2,1)} %wv.1, f32[1,1]{1,0:T(1,128)} %bitcast.6.mixing, ...), custom_call_target="tpu_custom_call" | custom-call | tf_op jit(solution)/shard_map/pallas_call | solution.py:363
  24.1 0.7 %copy.11 = bf16[32,2048]{1,0:T(8,128)(2,1)} copy(bf16[32,2048]{1,0:T(8,128)(2,1)S(1)} %shard_map.91) | data formatting | bytes 262144
